TPU v7x, 32 devices: a whole 2x2x4 slice. The times are simulated.
32 devices in a mesh: grp: 2 (over x), ep: 16 (over z, y, core).
Axes of the slice: x: 2, y: 2, z: 4, core: 2. Of those that a mesh axis runs over, the one named last changes fastest.
Arguments:
- residual: bfloat16 [16, 4096], P('grp', 'ep'), parts along dimension 0, may hold values from -6 to 6
- head_states: float32 [64, 512, 1024], P(('grp', 'ep')), parts along dimension 0, may hold values from -6 to 6
- first_gain: bfloat16 [4096], replicated, may hold values from 0.099609375 to 1.8984375
- w_query: bfloat16 [4096, 2048], P(None, 'ep'), may hold values from -0.09375 to 0.09375
- w_key: bfloat16 [4096, 2048], P(None, 'ep'), may hold values from -0.09375 to 0.09375
- w_value: bfloat16 [4096, 4096], P(None, 'ep'), may hold values from -0.09375 to 0.09375
- w_gate: bfloat16 [4096, 4096], P(None, 'ep'), may hold values from -0.09375 to 0.09375
- w_low: bfloat16 [4096, 16], replicated, may hold values from -0.09375 to 0.09375
- w_decay: bfloat16 [16, 2048], replicated, may hold values from -15 to 15
- decay_bias: float32 [2048], replicated, may hold values from -40 to 4
- head_gain: bfloat16 [1024], replicated, may hold values from 0.099609375 to 1.8984375
- w_output: bfloat16 [4096, 4096], P(None, 'ep'), may hold values from -0.09375 to 0.09375
- second_gain: bfloat16 [4096], replicated, may hold values from 0.099609375 to 1.8984375
- routes: int32 [16, 2], P('grp'), parts along dimension 0, may hold values from 0 to 15, as said below
- group_logits: float32 [16, 4], P('grp'), parts along dimension 0, may hold values from -12 to 12
- expert_logits: float32 [16, 2], P('grp'), parts along dimension 0, may hold values from -9 to 9
- expert_gate: bfloat16 [16, 4096, 512], P('ep'), may hold values from -0.09375 to 0.09375
- expert_up: bfloat16 [16, 4096, 512], P('ep'), may hold values from -0.09375 to 0.09375
- expert_down: bfloat16 [16, 512, 4096], P('ep'), may hold values from -0.25 to 0.25
Outputs:
- layer_out: bfloat16 [16, 4096], P('grp', 'ep'), parts along dimension 0
- new_states: float32 [64, 512, 1024], P(('grp', 'ep')), parts along dimension 0
There are 2 independent parts, one for each index of `grp`. A program takes and returns all parts, laid end to end along the dimension named above; an argument that names none is the same for every part. Nothing has to cross between parts.
Inputs may be any that keep to these rules, and one draw needn't show every extreme that they name: `routes`: each row names 2 different experts of one group (numbers g * 4 to g * 4 + 3). No expert is named by more than 2 rows, and in every draw all experts of one group are named by exactly 2 rows.
All inputs are finite; a program needn't handle non-finite values.
Results may differ from a plain program's by a relative error of at most 0.014.
Values may be sent and summed in bfloat16 or wider, within the bound.
A program may use at most 128 MiB of HBM per device.

v0:
```python
import jax
import jax.numpy as jnp
import numpy as np
from jax import lax
from jax.sharding import PartitionSpec as P

HEADS = 4
DK = 512
DV = 1024
GROUPS = 4
TOP = 2


norm_eps = 1e-06
decay_tau = 16.0


def rms_scale(values, gain):
    floats = values.astype(jnp.float32)
    return (
        floats
        * lax.rsqrt(jnp.mean(floats * floats, axis=-1, keepdims=True) + norm_eps)
        * gain.astype(jnp.float32)
    )


def route_weights(routes, group_logits, expert_logits, per_group):
    group_exp = jnp.exp(group_logits)
    group_prob = group_exp / jnp.sum(group_exp, axis=1, keepdims=True)
    chosen = routes[:, 0] // per_group
    groups_row = jnp.arange(group_logits.shape[1], dtype=jnp.int32)
    picked = jnp.sum(
        group_prob * (chosen[:, None] == groups_row[None, :]).astype(jnp.float32), axis=1
    )
    expert_exp = jnp.exp(expert_logits)
    return expert_exp / jnp.sum(expert_exp, axis=1, keepdims=True) * picked[:, None]


def per_device(
    residual,
    head_states,
    first_gain,
    w_query,
    w_key,
    w_value,
    w_gate,
    w_low,
    w_decay,
    decay_bias,
    head_gain,
    w_output,
    second_gain,
    routes,
    group_logits,
    expert_logits,
    expert_gate,
    expert_up,
    expert_down,
):
    devices = lax.axis_size("ep")
    my_index = lax.axis_index("ep")
    seq_count = residual.shape[0]
    own_width = residual.shape[1]
    width = own_width * devices
    pairs_dev = head_states.shape[0]
    slot_count = max(1, pairs_dev // HEADS)
    rows = lax.all_gather(residual, "ep", axis=1, tiled=True)
    normed = rms_scale(rows, first_gain).astype(jnp.bfloat16)
    my_head = my_index * HEADS // devices
    target = jnp.arange(devices, dtype=jnp.int32)[:, None]
    turn = jnp.arange(slot_count, dtype=jnp.int32)[None, :]
    within = jnp.mod(my_head - target * pairs_dev, HEADS) + turn * HEADS
    target_seq = (target * pairs_dev + within) // HEADS
    seq_row = jnp.arange(seq_count, dtype=jnp.int32)[None, None, :]
    picker = (target_seq[:, :, None] == seq_row) & (within < pairs_dev)[:, :, None]
    picker = picker.astype(jnp.bfloat16).reshape(devices * slot_count, seq_count)

    def outgoing(weight):
        projected = jnp.dot(normed, weight, preferred_element_type=jnp.float32).astype(jnp.bfloat16)
        placed = jnp.dot(picker, projected, preferred_element_type=jnp.float32).astype(jnp.bfloat16)
        return placed.reshape(devices, slot_count, projected.shape[1])

    send_query = outgoing(w_query)
    send_key = outgoing(w_key)
    send_value = outgoing(w_value)
    send_gate = outgoing(w_gate)
    incoming = (
        lax.all_to_all(send_query, "ep", split_axis=0, concat_axis=0, tiled=True),
        lax.all_to_all(send_key, "ep", split_axis=0, concat_axis=0, tiled=True),
        lax.all_to_all(send_value, "ep", split_axis=0, concat_axis=0, tiled=True),
        lax.all_to_all(send_gate, "ep", split_axis=0, concat_axis=0, tiled=True),
    )
    pair_ids = my_index * pairs_dev + jnp.arange(pairs_dev, dtype=jnp.int32)
    head_pick = (
        jnp.mod(pair_ids, HEADS)[:, None] == jnp.arange(HEADS, dtype=jnp.int32)[None, :]
    ).astype(jnp.bfloat16)
    turns = np.arange(pairs_dev) // HEADS
    pair_rows = np.arange(pairs_dev)

    def arrange(received):
        merged = jnp.dot(head_pick, received.reshape(HEADS, -1), preferred_element_type=jnp.float32)
        merged = merged.reshape(pairs_dev, devices // HEADS, slot_count, received.shape[2])
        return merged[pair_rows, :, turns, :].reshape(pairs_dev, -1).astype(jnp.bfloat16)

    query = arrange(incoming[0])
    key = arrange(incoming[1])
    value = arrange(incoming[2])
    gate = arrange(incoming[3])
    low = jnp.dot(normed, w_low, preferred_element_type=jnp.float32)
    decay_pre = (
        jnp.dot(low, w_decay.astype(jnp.float32), precision=lax.Precision.HIGHEST) + decay_bias
    )
    decay_pre = lax.dynamic_slice_in_dim(
        decay_pre.reshape(seq_count * HEADS, DK), my_index * pairs_dev, pairs_dev, 0
    )
    log_decay = jax.nn.log_sigmoid(decay_pre) / decay_tau
    new_states = (
        head_states * jnp.exp(log_decay)[:, :, None]
        + key.astype(jnp.float32)[:, :, None] * value.astype(jnp.float32)[:, None, :]
    )
    read = jnp.einsum(
        "pk,pkv->pv",
        query.astype(jnp.float32) * DK ** (-0.5),
        new_states,
        precision=lax.Precision.HIGHEST,
    )
    mixed = (rms_scale(read, head_gain) * jax.nn.silu(gate.astype(jnp.float32))).astype(
        jnp.bfloat16
    )
    gathered = lax.all_gather(mixed, "ep", axis=0, tiled=True).reshape(seq_count, HEADS * DV)
    branch = jnp.dot(gathered, w_output, preferred_element_type=jnp.float32).astype(jnp.bfloat16)
    stream = (residual.astype(jnp.float32) + branch.astype(jnp.float32)).astype(jnp.bfloat16)
    floats = stream.astype(jnp.float32)
    total = lax.psum(jnp.sum(floats * floats, axis=1), "ep")
    gain_part = lax.dynamic_slice_in_dim(second_gain, my_index * own_width, own_width)
    scaled = floats * lax.rsqrt(total / width + norm_eps)[:, None] * gain_part.astype(jnp.float32)
    expert_in = lax.all_gather(scaled.astype(jnp.bfloat16), "ep", axis=1, tiled=True)
    capacity = 2 * seq_count * TOP // devices
    weights = route_weights(routes, group_logits, expert_logits, devices // GROUPS)
    hits = (routes == my_index).astype(jnp.int32)
    mine = jnp.sum(weights * hits.astype(jnp.float32), axis=1)
    routed = jnp.sum(hits, axis=1)
    slot = jnp.cumsum(routed) - routed
    chooser = (slot[None, :] == jnp.arange(capacity, dtype=jnp.int32)[:, None]) & (
        routed[None, :] > 0
    )
    picked = jnp.dot(
        chooser.astype(jnp.bfloat16), expert_in, preferred_element_type=jnp.float32
    ).astype(jnp.bfloat16)
    row_weight = jnp.dot(chooser.astype(jnp.float32), mine, precision=lax.Precision.HIGHEST)
    gate_part = jnp.dot(picked, expert_gate[0], preferred_element_type=jnp.float32)
    up_part = jnp.dot(picked, expert_up[0], preferred_element_type=jnp.float32)
    active = (jax.nn.silu(gate_part) * up_part * row_weight[:, None]).astype(jnp.bfloat16)
    expert_rows = jnp.dot(active, expert_down[0], preferred_element_type=jnp.float32).astype(
        jnp.bfloat16
    )
    arrived = lax.all_to_all(expert_rows, "ep", split_axis=1, concat_axis=0, tiled=True)
    every = jnp.arange(devices, dtype=jnp.int32)
    hit_all = jnp.sum((routes[:, :, None] == every[None, None, :]).astype(jnp.int32), axis=1)
    slot_all = jnp.cumsum(hit_all, axis=0) - hit_all
    placer = (slot_all[:, :, None] == jnp.arange(capacity, dtype=jnp.int32)[None, None, :]) & (
        hit_all[:, :, None] > 0
    )
    placer = placer.astype(jnp.bfloat16).reshape(seq_count, devices * capacity)
    returned = jnp.dot(placer, arrived, preferred_element_type=jnp.float32)
    layer_out = (stream.astype(jnp.float32) + returned).astype(jnp.bfloat16)
    return (layer_out, new_states)


def solution(mesh):
    return jax.shard_map(
        per_device,
        mesh=mesh,
        in_specs=(
            P("grp", "ep"),
            P(("grp", "ep"), None, None),
            P(),
            P(None, "ep"),
            P(None, "ep"),
            P(None, "ep"),
            P(None, "ep"),
            P(),
            P(),
            P(),
            P(),
            P(None, "ep"),
            P(),
            P("grp", None),
            P("grp", None),
            P("grp", None),
            P("ep", None, None),
            P("ep", None, None),
            P("ep", None, None),
        ),
        out_specs=(P("grp", "ep"), P(("grp", "ep"), None, None)),
        check_vma=False,
    )
```

profile of v0, /device:TPU:0, one launch (start us, length us, event | category | flops | bytes accessed | tf_op | source)
XLA Modules:
  0.0 169.2 jit_solution(12246803465482614124)
XLA Ops:
  0.6 0.0 copy-start
  0.6 0.0 copy-start.3
  0.7 0.0 copy-start.4
  0.7 0.0 copy-start.6
  0.7 0.0 copy-start.5
  0.7 23.7 %all_gather.9 = bf16[8,4096]{1,0:T(8,128)(2,1)S(1)} all-gather(bf16[8,256]{1,0:T(8,128)(2,1)} %param.29), channel_id=1, replica_groups=mesh['grp'=2,'ep'=16] {'ep'}, dimensions={1}, use_global_device_ids=true | all-gather | bytes 69632 | tf_op jit(solution)/shard_map/all_gather | solution.py:67
  24.4 0.1 fusion.26
  24.6 0.7 convert_element_type.145
  25.3 1.6 fusion.14
  26.9 0.6 copy.61
  27.5 3.4 %all-to-all-start.1 = ((bf16[16,1,128]{2,1,0:T(2,128)(2,1)}), bf16[16,1,128]{2,1,0:T(2,128)(2,1)S(1)}, u32[]{:S(2)}, u32[]{:S(2)}) async-start(bf16[16,1,128]{2,1,0:T(2,128)(2,1)} %copy.61), calls=%async_computation.1 | async-start | bytes 16384 | tf_op jit(solution)/shard_map/all_to_all | solution.py:89
  31.0 0.7 fusion.70
  31.7 0.7 fusion.73
  32.4 0.8 convert_reduce_fusion
  33.1 0.5 fusion.5
  33.6 1.1 fusion.88
  34.8 1.0 convolution_add_fusion
  35.8 1.6 fusion.13
  37.4 2.1 %fusion.6 = bf16[16,1,256]{2,0,1:T(8,128)(2,1)S(1)} fusion(bf16[4096,256]{1,0:T(8,128)(2,1)} %param.35, s32[16]{0:T(128)S(1)} %and_select_fusion.1, pred[16]{0:T(512)(128)(4,1)S(1)} %broadcast_compare_fusion.2, bf16[8,4096]{1,0:T(8,128)(2,1)S(1)} %all_gather.9, f32[4096]{0:T(1024)S(1)} %convert_element_type.145, f32[8]{0:T(128)S(1)} %add_rsqrt_fusion.2), kind=kOutput, calls=%fused_computation.16 | convolution fusion | flops 16980224 | bytes 2187376 | tf_op jit(solution)/shard_map/dot_general | solution.py:80
  39.6 0.2 reduce-window.8
  39.8 0.0 copy-done.6
  39.9 0.8 dynamic-slice_convert_fusion
  40.7 0.1 convolution_bitcast_fusion.5
  40.8 0.5 broadcast.372
  41.3 0.6 reduce.5
  42.0 0.6 reshape.330
  42.6 0.6 copy.59
  43.2 0.6 reduce.4
  43.9 0.6 reshape.328
  44.5 0.0 all-to-all-done.1
  44.5 6.0 %all-to-all-start = ((bf16[16,1,128]{2,1,0:T(2,128)(2,1)}), bf16[16,1,128]{2,1,0:T(2,128)(2,1)S(1)}, u32[]{:S(2)}, u32[]{:S(2)}) async-start(bf16[16,1,128]{2,1,0:T(2,128)(2,1)} %copy.59), calls=%async_computation | async-start | bytes 16384 | tf_op jit(solution)/shard_map/all_to_all | solution.py:88
  50.5 0.2 convolution_bitcast_fusion.3
  50.7 0.6 gather_fusion.1
  51.3 5.5 %all-to-all-done = bf16[16,1,128]{2,1,0:T(2,128)(2,1)S(1)} async-done(((bf16[16,1,128]{2,1,0:T(2,128)(2,1)}), bf16[16,1,128]{2,1,0:T(2,128)(2,1)S(1)}, u32[]{:S(2)}, u32[]{:S(2)}) %all-to-all-start) | async-done | bytes 4128 | tf_op jit(solution)/shard_map/all_to_all | solution.py:88
  56.8 3.4 %all-to-all-start.2 = ((bf16[16,2,128]{2,1,0:T(2,128)(2,1)}), bf16[16,2,128]{2,1,0:T(2,128)(2,1)S(1)}, u32[]{:S(2)}, u32[]{:S(2)}) async-start(bf16[16,2,128]{2,1,0:T(2,128)(2,1)} %reshape.330), calls=%async_computation.2 | async-start | bytes 16384 | tf_op jit(solution)/shard_map/all_to_all | solution.py:90
  60.3 0.2 convolution_bitcast_fusion.4
  60.5 0.6 gather_fusion
  61.1 5.6 %all-to-all-done.2 = bf16[16,2,128]{2,1,0:T(2,128)(2,1)S(1)} async-done(((bf16[16,2,128]{2,1,0:T(2,128)(2,1)}), bf16[16,2,128]{2,1,0:T(2,128)(2,1)S(1)}, u32[]{:S(2)}, u32[]{:S(2)}) %all-to-all-start.2) | async-done | bytes 8224 | tf_op jit(solution)/shard_map/all_to_all | solution.py:90
  66.6 3.5 %all-to-all-start.3 = ((bf16[16,2,128]{2,1,0:T(2,128)(2,1)}), bf16[16,2,128]{2,1,0:T(2,128)(2,1)S(1)}, u32[]{:S(2)}, u32[]{:S(2)}) async-start(bf16[16,2,128]{2,1,0:T(2,128)(2,1)} %reshape.328), calls=%async_computation.3 | async-start | bytes 16384 | tf_op jit(solution)/shard_map/all_to_all | solution.py:91
  70.1 0.1 reduce.2
  70.2 0.2 convolution_bitcast_fusion.2
  70.4 0.6 gather_fusion.2
  71.0 2.7 %multiply_add_fusion = f32[2,512,1024]{2,1,0:T(8,128)S(1)} fusion(f32[2,512,1024]{2,1,0:T(8,128)} %param.30, f32[2,1024]{1,0:T(2,128)S(1)} %bitcast.122, f32[2,512]{1,0:T(2,128)S(1)} %bitcast.124, f32[2,512]{1,0:T(2,128)S(1)} %fusion.44), kind=kLoop, calls=%fused_computation.11 | loop fusion | flops 3145728 | bytes 8404992 | tf_op jit(solution)/shard_map/add | solution.py:118
  73.7 0.0 copy-start.1
  73.8 0.0 copy-start.2
  73.8 2.0 %copy-done.1 = f32[2,512,1024]{2,1,0:T(8,128)} copy-done((f32[2,512,1024]{2,1,0:T(8,128)}, f32[2,512,1024]{2,1,0:T(8,128)S(1)}, u32[]{:S(2)}) %copy-start.1) | copy-done | bytes 4194328
  75.8 2.1 %fusion.92 = f32[2,1,1024]{2,1,0:T(1,128)S(1)} fusion(f32[2,512,1]{1,2,0:T(1,128)S(1)} %bitcast.123, f32[2,512,1024]{2,1,0:T(8,128)S(1)} %multiply_add_fusion), kind=kOutput, calls=%fused_computation.142 | convolution fusion | flops 12582912 | bytes 4206592 | tf_op jit(solution)/shard_map/pk,pkv->pv/dot_general | solution.py:121
  77.8 0.1 fusion.32
  78.0 0.0 all-to-all-done.3
  78.0 0.1 reduce.3
  78.1 0.2 convolution_bitcast_fusion.1
  78.3 0.6 gather_fusion.3
  78.9 0.1 fusion.60
  78.9 21.8 %all-gather = bf16[16,2,1024]{2,1,0:T(2,128)(2,1)S(1)} all-gather(bf16[1,2,1024]{2,1,0:T(2,128)(2,1)S(1)} %fusion.60), channel_id=1, replica_groups=mesh['grp'=2,'ep'=16] {'ep'}, dimensions={0}, use_global_device_ids=true | all-gather | bytes 69632 | tf_op jit(solution)/shard_map/all_gather | solution.py:130
  100.8 2.1 %multiply_reduce_fusion = (f32[8]{0:T(128)S(1)}, f32[8,256]{1,0:T(8,128)S(1)}) fusion(bf16[8,4096]{1,0:T(8,128)(2,1)S(1)} %reshape.284, bf16[4096,256]{1,0:T(8,128)(2,1)} %param.40, bf16[8,256]{1,0:T(8,128)(2,1)S(1)} %copy-done.2), kind=kOutput, calls=%fused_computation.58 | convolution fusion | flops 16793592 | bytes 2175008 | tf_op jit(solution)/shard_map/dot_general | solution.py:131
  102.9 29.8 %psum.7 = f32[8]{0:T(128)S(1)} all-reduce(f32[8]{0:T(128)S(1)} %get-tuple-element.2), channel_id=1, replica_groups=mesh['grp'=2,'ep'=16] {'ep'}, use_global_device_ids=true, to_apply=%region_7.8 | all-reduce | flops 8 | bytes 64 | tf_op jit(solution)/shard_map/psum | solution.py:134
  132.7 0.1 multiply_convert_fusion
  132.8 17.3 %all_gather.11 = bf16[8,4096]{1,0:T(8,128)(2,1)S(1)} all-gather(bf16[8,256]{1,0:T(8,128)(2,1)S(1)} %multiply_convert_fusion), channel_id=1, replica_groups=mesh['grp'=2,'ep'=16] {'ep'}, dimensions={1}, use_global_device_ids=true | all-gather | bytes 69632 | tf_op jit(solution)/shard_map/all_gather | solution.py:137
  150.1 0.1 convolution_convert_fusion.1
  150.2 2.8 %fusion.3 = f32[2,512]{1,0:T(2,128)S(1)} fusion(bf16[2,4096]{1,0:T(2,128)(2,1)S(1)} %convolution_convert_fusion.1, bf16[1,4096,512]{2,1,0:T(8,128)(2,1)} %param.45), kind=kOutput, calls=%fused_computation.9 | convolution fusion | flops 8388608 | bytes 4214784 | tf_op jit(solution)/shard_map/dot_general | solution.py:151
  153.1 5.4 %convolution_convert_fusion = bf16[2,4096]{1,0:T(2,128)(2,1)} fusion(bf16[1,512,4096]{2,1,0:T(8,128)(2,1)} %param.47, bf16[2,4096]{1,0:T(2,128)(2,1)S(1)} %convolution_convert_fusion.1, bf16[1,4096,512]{2,1,0:T(8,128)(2,1)} %param.46, f32[2,512]{1,0:T(2,128)S(1)} %fusion.3, f32[2]{0:T(128)S(1)} %convolution_bitcast_fusion.5), kind=kOutput, calls=%fused_computation.4 | convolution fusion | flops 16792576 | bytes 8425480 | tf_op jit(solution)/shard_map/dot_general | solution.py:154
  158.4 3.5 %all-to-all-start.4 = ((bf16[2,16,256]{2,0,1:T(2,128)(2,1)}), bf16[2,16,256]{2,0,1:T(2,128)(2,1)S(1)}, u32[]{:S(2)}, u32[]{:S(2)}) async-start(bf16[2,16,256]{2,0,1:T(2,128)(2,1)} %bitcast.28), calls=%async_computation.4 | async-start | bytes 32768 | tf_op jit(solution)/shard_map/all_to_all | solution.py:157
  162.0 6.4 %all-to-all-done.4 = bf16[2,16,256]{2,0,1:T(2,128)(2,1)S(1)} async-done(((bf16[2,16,256]{2,0,1:T(2,128)(2,1)}), bf16[2,16,256]{2,0,1:T(2,128)(2,1)S(1)}, u32[]{:S(2)}, u32[]{:S(2)}) %all-to-all-start.4) | async-done | bytes 16416 | tf_op jit(solution)/shard_map/all_to_all | solution.py:157
  168.4 0.8 fusion.8
  (44 shorter events, 0.5 us)
Async XLA Ops:
  0.6 32.5 %copy-start = (bf16[4096,256]{1,0:T(8,128)(2,1)S(1)}, bf16[4096,256]{1,0:T(8,128)(2,1)}, u32[]{:S(2)}) copy-start(bf16[4096,256]{1,0:T(8,128)(2,1)} %param.34) | copy-start | bytes 6291460
  0.6 40.0 %copy-start.3 = (s32[8,2]{0,1:T(2,128)S(1)}, s32[8,2]{0,1:T(2,128)}, u32[]{:S(2)}) copy-start(s32[8,2]{0,1:T(2,128)} %param.42) | copy-start | bytes 196
  0.7 39.1 %copy-start.4 = (f32[8,4]{0,1:T(4,128)S(1)}, f32[8,4]{0,1:T(4,128)}, u32[]{:S(2)}) copy-start(f32[8,4]{0,1:T(4,128)} %param.43) | copy-start | bytes 388
  0.7 39.1 %copy-start.6 = (f32[8,2]{0,1:T(2,128)S(1)}, f32[8,2]{0,1:T(2,128)}, u32[]{:S(2)}) copy-start(f32[8,2]{0,1:T(2,128)} %param.44) | copy-start | bytes 196
  0.7 43.8 %copy-start.5 = (bf16[1024]{0:T(1024)(128)(2,1)S(1)}, bf16[1024]{0:T(1024)(128)(2,1)}, u32[]{:S(2)}) copy-start(bf16[1024]{0:T(1024)(128)(2,1)} %param.39) | copy-start | bytes 6148
  27.5 16.9 %all-to-all-start.1 = ((bf16[16,1,128]{2,1,0:T(2,128)(2,1)}), bf16[16,1,128]{2,1,0:T(2,128)(2,1)S(1)}, u32[]{:S(2)}, u32[]{:S(2)}) async-start(bf16[16,1,128]{2,1,0:T(2,128)(2,1)} %copy.61), calls=%async_computation.1 | async-start | bytes 16384 | tf_op jit(solution)/shard_map/all_to_all | solution.py:89
  44.5 12.3 %all-to-all-start = ((bf16[16,1,128]{2,1,0:T(2,128)(2,1)}), bf16[16,1,128]{2,1,0:T(2,128)(2,1)S(1)}, u32[]{:S(2)}, u32[]{:S(2)}) async-start(bf16[16,1,128]{2,1,0:T(2,128)(2,1)} %copy.59), calls=%async_computation | async-start | bytes 16384 | tf_op jit(solution)/shard_map/all_to_all | solution.py:88
  56.8 9.8 %all-to-all-start.2 = ((bf16[16,2,128]{2,1,0:T(2,128)(2,1)}), bf16[16,2,128]{2,1,0:T(2,128)(2,1)S(1)}, u32[]{:S(2)}, u32[]{:S(2)}) async-start(bf16[16,2,128]{2,1,0:T(2,128)(2,1)} %reshape.330), calls=%async_computation.2 | async-start | bytes 16384 | tf_op jit(solution)/shard_map/all_to_all | solution.py:90
  66.6 11.3 %all-to-all-start.3 = ((bf16[16,2,128]{2,1,0:T(2,128)(2,1)}), bf16[16,2,128]{2,1,0:T(2,128)(2,1)S(1)}, u32[]{:S(2)}, u32[]{:S(2)}) async-start(bf16[16,2,128]{2,1,0:T(2,128)(2,1)} %reshape.328), calls=%async_computation.3 | async-start | bytes 16384 | tf_op jit(solution)/shard_map/all_to_all | solution.py:91
  73.7 2.0 %copy-start.1 = (f32[2,512,1024]{2,1,0:T(8,128)}, f32[2,512,1024]{2,1,0:T(8,128)S(1)}, u32[]{:S(2)}) copy-start(f32[2,512,1024]{2,1,0:T(8,128)S(1)} %multiply_add_fusion) | copy-start | bytes 12582916
  73.8 27.0 %copy-start.2 = (bf16[8,256]{1,0:T(8,128)(2,1)S(1)}, bf16[8,256]{1,0:T(8,128)(2,1)}, u32[]{:S(2)}) copy-start(bf16[8,256]{1,0:T(8,128)(2,1)} %param.29) | copy-start | bytes 12292
  158.4 10.0 %all-to-all-start.4 = ((bf16[2,16,256]{2,0,1:T(2,128)(2,1)}), bf16[2,16,256]{2,0,1:T(2,128)(2,1)S(1)}, u32[]{:S(2)}, u32[]{:S(2)}) async-start(bf16[2,16,256]{2,0,1:T(2,128)(2,1)} %bitcast.28), calls=%async_computation.4 | async-start | bytes 32768 | tf_op jit(solution)/shard_map/all_to_all | solution.py:157
where the time goes:
time: 170 us; the launch traced here: 169 us
  blocking collectives  92.6 us (54%)
  matrix products  22.2 us (13%)
  starting transfers between devices  19.8 us (12%)
  waiting for transfers between devices  17.5 us (10%)
  other arithmetic  8.69 us (5%)
  local copies, waits for them, and re-layouts  7.43 us (4%)
    psum x1, blocking collectives, per_device(): total = lax.psum(jnp.sum(floats * floats, axis=1), 'ep')  29.8 us
    all_gather x1, blocking collectives, per_device(): rows = lax.all_gather(residual, 'ep', axis=1, tiled=True)  23.7 us
    all_gather x1, blocking collectives, per_device(): lax.all_gather(mixed, 'ep', axis=0, tiled=True)  21.8 us
    all_gather x1, blocking collectives, per_device(): lax.all_gather(scaled.astype(jnp.bfloat16), 'ep', axis=1, tiled=True)  17.3 us
    all_to_all x1, waiting for transfers between devices, per_device(): lax.all_to_all(expert_rows, 'ep', split_axis=1, concat_axis=0, tiled=True)  6.42 us
    all_to_all x1, starting transfers between devices, per_device(): lax.all_to_all(send_query, 'ep', split_axis=0, concat_axis=0, tiled=True)  5.98 us
    dot_general x4, matrix products, outgoing(): jnp.dot(picker, projected, preferred_element_type=jnp.float32)  5.92 us
    all_to_all x1, waiting for transfers between devices, per_device(): lax.all_to_all(send_value, 'ep', split_axis=0, concat_axis=0, tiled=True)  5.56 us
  transfers between devices with their start and end apart: 5, of which 3 were waited for; matrix products, arithmetic and copies ran while one was open for 12% of the time, Pallas kernels for 0%

commit v1 on v0

v1 whole, which is shorter than its diff:
```python
import functools

import jax
import jax.numpy as jnp
from jax import lax
from jax.experimental import pallas as pl
from jax.experimental.pallas import tpu as pltpu
from jax.sharding import PartitionSpec as P

HEADS = 4
DK = 512
DV = 1024
GROUPS = 4

NORM_EPS = 1e-06
DECAY_TAU = 16.0
MESH = pl.DeviceIdType.MESH
F32 = jnp.float32
BF16 = jnp.bfloat16


def kernel_body(n, *refs):
    (
        residual,
        head_states,
        first_gain,
        w_query,
        w_key,
        w_value,
        w_gate,
        w_low,
        w_decay,
        decay_bias,
        head_gain,
        w_output,
        second_gain,
        routes,
        group_logits,
        expert_logits,
        expert_gate,
        expert_up,
        expert_down,
        layer_out,
        new_states,
        res_v,
        states_v,
        gain1_v,
        wq_v,
        wk_v,
        wv_v,
        wg_v,
        wlow_v,
        wdec_v,
        bias_v,
        hgain_v,
        wout_v,
        gain2_v,
        routes_v,
        glog_v,
        elog_v,
        eg_v,
        eu_v,
        ed_v,
        gath1,
        lhs,
        send2,
        recv2,
        cols,
        send3,
        gath3,
        stage3,
        stream_v,
        gath4,
        send5,
        recv5,
        out_v,
        local_sem,
        out_sem,
        s1,
        r1,
        s2,
        r2,
        s3,
        r3,
        s4,
        r4,
        s5,
        r5,
    ) = refs
    me = lax.axis_index("ep")
    seqs, own = residual.shape
    width = own * n
    pairs_dev = head_states.shape[0]
    dph = n // HEADS
    qw, vw = w_query.shape[1], w_value.shape[1]
    group_src = pairs_dev * dph
    my_seq = me * pairs_dev // HEADS
    my_head0 = lax.rem(me * pairs_dev, HEADS)
    src_head = me // dph
    tiles2 = send2.shape[1]
    rows3 = send3.shape[0]

    pieces = [
        (residual, res_v),
        (first_gain, gain1_v),
        (w_query, wq_v),
        (w_key, wk_v),
        (w_value, wv_v),
        (w_gate, wg_v),
        (w_low, wlow_v),
        (w_decay, wdec_v),
        (decay_bias, bias_v),
        (head_states, states_v),
        (head_gain, hgain_v),
        (w_output, wout_v),
        (second_gain, gain2_v),
        (routes, routes_v),
        (group_logits, glog_v),
        (expert_logits, elog_v),
        (expert_gate, eg_v),
        (expert_up, eu_v),
        (expert_down, ed_v),
    ]
    copies = [
        pltpu.make_async_copy(src, dst, local_sem.at[i]) for i, (src, dst) in enumerate(pieces)
    ]
    for copy in copies:
        copy.start()

    def staged(*indices):
        for i in indices:
            copies[i].wait()

    barrier = pltpu.get_barrier_semaphore()

    @pl.loop(1, n)
    def _(o):
        pl.semaphore_signal(
            barrier, inc=1, device_id={"ep": lax.rem(me + o, n)}, device_id_type=MESH
        )

    staged(0)
    pl.semaphore_wait(barrier, n - 1)

    def spread(src, dst_of_me, send_sem, recv_sem):
        def one(o):
            t = lax.rem(me + o, n)
            return pltpu.make_async_remote_copy(
                src_ref=src,
                dst_ref=dst_of_me,
                send_sem=send_sem.at[o],
                recv_sem=recv_sem.at[me],
                device_id={"ep": t},
                device_id_type=MESH,
            )

        @pl.loop(1, n)
        def _(o):
            one(o).start()

    def drain(src, buffer, send_sem, recv_sem):
        @pl.loop(1, n)
        def _(o):
            s = lax.rem(me + o, n)
            pltpu.make_async_copy(src, buffer.at[s], recv_sem.at[s]).wait()

    def drain_sends(src, buffer, send_sem):
        @pl.loop(1, n)
        def _(o):
            pltpu.make_async_copy(src, buffer.at[0], send_sem.at[o]).wait()

    spread(res_v, gath1.at[me], s1, r1)
    gath1[me] = res_v[...]
    drain(res_v, gath1, s1, r1)
    staged(1)

    def normalise(gath, gain):
        total = jnp.zeros((seqs, own), F32)
        for s in range(n):
            x = gath[s].astype(F32)
            total = total + x * x
        scale = lax.rsqrt(jnp.sum(total, axis=1, keepdims=True) / width + NORM_EPS)
        for s in range(n):
            g = gain[:, s * own : (s + 1) * own].astype(F32)
            lhs[:, s * own : (s + 1) * own] = (gath[s].astype(F32) * scale * g).astype(BF16)

    normalise(gath1, gain1_v)

    def kdot(weights, chunk):
        depth = lhs.shape[1]
        outs = tuple(jnp.zeros((seqs, w.shape[1]), F32) for w in weights)

        def step(i, accs):
            at = pl.ds(pl.multiple_of(i * chunk, chunk), chunk)
            x = lhs[:, at]
            return tuple(
                acc + jnp.dot(x, w[at, :], preferred_element_type=F32)
                for acc, w in zip(accs, weights)
            )

        return lax.fori_loop(0, depth // chunk, step, outs)

    staged(2, 3, 4, 5)
    q, k, v, g = kdot((wq_v, wk_v, wv_v, wg_v), 512)
    row = jnp.concatenate([q, k, v, g], axis=1).astype(BF16).astype(F32)
    for c in range(tiles2):
        part = row[:, c * 128 : (c + 1) * 128]
        for s in range(seqs):
            send2[s, c : c + 1, :] = part[s : s + 1, :]

    my_slot = lax.rem(me, group_src)

    def target2(s):
        return (s * HEADS + src_head) // pairs_dev

    def copy2(s):
        return pltpu.make_async_remote_copy(
            src_ref=send2.at[s],
            dst_ref=recv2.at[my_slot],
            send_sem=s2.at[s],
            recv_sem=r2.at[my_slot],
            device_id={"ep": target2(s)},
            device_id_type=MESH,
        )

    @pl.loop(0, seqs)
    def _(s):
        @pl.when(target2(s) != me)
        def _():
            copy2(s).start()

        @pl.when(target2(s) == me)
        def _():
            pltpu.make_async_copy(send2.at[s], recv2.at[my_slot], r2.at[my_slot]).start()

    staged(6, 7, 8)
    (low,) = kdot((wlow_v,), 1024)
    head_at = pl.ds(pl.multiple_of(my_head0 * DK, DK), pairs_dev * DK)
    pre = jnp.dot(
        low,
        wdec_v[:, head_at].astype(F32),
        preferred_element_type=F32,
        precision=lax.Precision.HIGHEST,
    )
    row_is = lax.broadcasted_iota(jnp.int32, pre.shape, 0) == my_seq
    pre = jnp.sum(jnp.where(row_is, pre, 0.0), axis=0, keepdims=True) + bias_v[:, head_at]
    log_sig = jnp.minimum(pre, 0.0) - jnp.log(1.0 + jnp.exp(-jnp.abs(pre)))
    decay = jnp.exp(log_sig / DECAY_TAU)

    @pl.loop(0, group_src)
    def _(i):
        pltpu.make_async_copy(send2.at[0], recv2.at[i], r2.at[i]).wait()

    def lanes(i, start, size):
        out = []
        while size:
            c, off = start // 128, start % 128
            take = min(size, 128 - off)
            out.append(recv2[i, c : c + 1, :][:, off : off + take])
            start, size = start + take, size - take
        return out

    def gathered_row(p, start, size):
        out = []
        for i in range(dph):
            out.extend(lanes(p * dph + i, start, size))
        return jnp.concatenate(out, axis=1)

    stack = []
    for p in range(pairs_dev):
        stack.append(gathered_row(p, 0, qw) * DK ** (-0.5))
        stack.append(gathered_row(p, qw, qw))
        stack.append(decay[:, p * DK : (p + 1) * DK])
    stack.append(jnp.zeros((8 - len(stack), DK), F32))
    cols[...] = jnp.transpose(jnp.concatenate(stack, axis=0))
    staged(9, 10)
    step_rows = 32
    mixed_rows = []
    for p in range(pairs_dev):
        value = gathered_row(p, 2 * qw, vw)

        def update(i, acc):
            at = pl.ds(pl.multiple_of(i * step_rows, step_rows), step_rows)
            three = cols[at, 3 * p : 3 * p + 3]
            fresh = states_v[p, at, :] * three[:, 2:3] + three[:, 1:2] * value
            states_v[p, at, :] = fresh
            weighted = fresh * three[:, 0:1]
            return acc + jnp.sum(weighted.reshape(step_rows // 8, 8, DV), axis=0)

        acc = lax.fori_loop(0, DK // step_rows, update, jnp.zeros((8, DV), F32))
        pltpu.make_async_copy(states_v.at[p], new_states.at[p], out_sem.at[p]).start()
        read = jnp.sum(acc, axis=0, keepdims=True)
        gate = gathered_row(p, 2 * qw + vw, vw)
        scale = lax.rsqrt(jnp.mean(read * read, axis=1, keepdims=True) + NORM_EPS)
        mixed = read * scale * hgain_v[...].astype(F32) * (gate / (1.0 + jnp.exp(-gate)))
        mixed_rows.extend(mixed[:, c * 128 : (c + 1) * 128] for c in range(DV // 128))
    send3[...] = jnp.concatenate(mixed_rows, axis=0).astype(BF16)

    spread(send3, gath3.at[me], s3, r3)
    gath3[me] = send3[...]
    drain(send3, gath3, s3, r3)
    per_seq = HEADS // pairs_dev
    for d in range(n):
        stage3[d // per_seq, (d % per_seq) * rows3 : (d % per_seq + 1) * rows3, :] = gath3[
            d
        ].astype(F32)
    for c in range(HEADS * DV // 128):
        lhs[:, c * 128 : (c + 1) * 128] = stage3[:, c, :].astype(BF16)
    staged(11)
    (branch,) = kdot((wout_v,), 1024)
    stream = (res_v[...].astype(F32) + branch.astype(BF16).astype(F32)).astype(BF16)
    stream_v[...] = stream

    spread(stream_v, gath4.at[me], s4, r4)
    gath4[me] = stream
    staged(12, 13, 14, 15)
    group_exp = jnp.exp(glog_v[...])
    group_prob = group_exp / jnp.sum(group_exp, axis=1, keepdims=True)
    route = routes_v[...]
    chosen = route[:, 0:1] // (n // GROUPS)
    group_is = lax.broadcasted_iota(jnp.int32, group_prob.shape, 1) == chosen
    picked = jnp.sum(jnp.where(group_is, group_prob, 0.0), axis=1, keepdims=True)
    expert_exp = jnp.exp(elog_v[...])
    weights = expert_exp / jnp.sum(expert_exp, axis=1, keepdims=True) * picked
    mine = jnp.sum(jnp.where(route == me, weights, 0.0), axis=1, keepdims=True)
    drain(stream_v, gath4, s4, r4)
    normalise(gath4, gain2_v)
    staged(16, 17)
    gate_part, up_part = kdot((eg_v.at[0], eu_v.at[0]), 512)
    active = (gate_part / (1.0 + jnp.exp(-gate_part)) * up_part * mine).astype(BF16)
    staged(18)

    def copy5(o):
        t = lax.rem(me + o, n)
        return pltpu.make_async_remote_copy(
            src_ref=send5.at[o],
            dst_ref=recv5.at[me],
            send_sem=s5.at[o],
            recv_sem=r5.at[me],
            device_id={"ep": t},
            device_id_type=MESH,
        )

    def contribution(t):
        at = pl.ds(pl.multiple_of(t * own, own), own)
        return jnp.dot(active, ed_v[0, :, at], preferred_element_type=F32).astype(BF16)

    @pl.loop(1, n)
    def _(o):
        send5[o] = contribution(lax.rem(me + o, n))
        copy5(o).start()

    recv5[me] = contribution(me)
    drain(stream_v, recv5, s5, r5)
    total = jnp.zeros((seqs, own), F32)
    for s in range(n):
        total = total + recv5[s].astype(F32)
    out_v[...] = (stream.astype(F32) + total).astype(BF16)
    out_copy = pltpu.make_async_copy(out_v, layer_out, out_sem.at[pairs_dev])
    out_copy.start()

    drain_sends(res_v, gath1, s1)
    drain_sends(send3, gath3, s3)
    drain_sends(stream_v, gath4, s4)
    drain_sends(stream_v, recv5, s5)

    @pl.loop(0, seqs)
    def _(s):
        @pl.when(target2(s) != me)
        def _():
            copy2(s).wait_send()

    for p in range(pairs_dev):
        pltpu.make_async_copy(states_v.at[p], new_states.at[p], out_sem.at[p]).wait()
    out_copy.wait()


def per_device(*args):
    n = lax.axis_size("ep")
    args = list(args)
    for i in (2, 9, 10, 12):
        args[i] = args[i].reshape(1, -1)
    residual, head_states = args[0], args[1]
    seqs, own = residual.shape
    pairs_dev = head_states.shape[0]
    width = own * n
    qw, vw = args[3].shape[1], args[5].shape[1]
    group_src = pairs_dev * (n // HEADS)
    tiles2 = (2 * qw + 2 * vw) // 128
    rows3 = pairs_dev * DV // 128
    dma = pltpu.SemaphoreType.DMA
    stage = [pltpu.VMEM(a.shape, a.dtype) for a in args]
    return pl.pallas_call(
        functools.partial(kernel_body, n),
        out_shape=(
            jax.ShapeDtypeStruct(residual.shape, BF16),
            jax.ShapeDtypeStruct(head_states.shape, F32),
        ),
        in_specs=[pl.BlockSpec(memory_space=pl.ANY)] * len(args),
        out_specs=(pl.BlockSpec(memory_space=pl.ANY),) * 2,
        scratch_shapes=stage
        + [
            pltpu.VMEM((n, seqs, own), BF16),
            pltpu.VMEM((seqs, width), BF16),
            pltpu.VMEM((seqs, tiles2, 128), F32),
            pltpu.VMEM((group_src, tiles2, 128), F32),
            pltpu.VMEM((DK, 8), F32),
            pltpu.VMEM((rows3, 128), BF16),
            pltpu.VMEM((n, rows3, 128), BF16),
            pltpu.VMEM((seqs, HEADS * DV // 128, 128), F32),
            pltpu.VMEM((seqs, own), BF16),
            pltpu.VMEM((n, seqs, own), BF16),
            pltpu.VMEM((n, seqs, own), BF16),
            pltpu.VMEM((n, seqs, own), BF16),
            pltpu.VMEM((seqs, own), BF16),
            dma((len(args),)),
            dma((pairs_dev + 1,)),
            dma((n,)),
            dma((n,)),
            dma((seqs,)),
            dma((group_src,)),
            dma((n,)),
            dma((n,)),
            dma((n,)),
            dma((n,)),
            dma((n,)),
            dma((n,)),
        ],
        compiler_params=pltpu.CompilerParams(
            collective_id=0, has_side_effects=True, vmem_limit_bytes=56 * 1024 * 1024
        ),
        name="layer",
    )(*args)


def solution(mesh):
    return jax.shard_map(
        per_device,
        mesh=mesh,
        in_specs=(
            P("grp", "ep"),
            P(("grp", "ep"), None, None),
            P(),
            P(None, "ep"),
            P(None, "ep"),
            P(None, "ep"),
            P(None, "ep"),
            P(),
            P(),
            P(),
            P(),
            P(None, "ep"),
            P(),
            P("grp", None),
            P("grp", None),
            P("grp", None),
            P("ep", None, None),
            P("ep", None, None),
            P("ep", None, None),
        ),
        out_specs=(P("grp", "ep"), P(("grp", "ep"), None, None)),
        check_vma=False,
    )
```

time: 170 us -> 54 us (0.32)
  blocking collectives: 92.6 us -> 0 us
  Pallas kernels: 0 us -> 36.8 us
  matrix products: 22.2 us -> 0 us
  starting transfers between devices: 19.8 us -> 0 us
  waiting for transfers between devices: 17.5 us -> 0 us
  local copies, waits for them, and re-layouts: 7.43 us -> 16.2 us
  other arithmetic: 8.69 us -> 0 us
    all_gather x3 -> x0, blocking collectives: 62.8 us -> none  [the longest x1 23.7 us: per_device(): rows = lax.all_gather(residual, 'ep', axis=1, tiled=True)]
    pallas_call x0 -> x1, Pallas kernels: none -> 36.8 us  [per_device(): pl.pallas_call(functools.partial(kernel_body, n), out_shape=(jax.ShapeDty...]
    psum x1 -> x0, blocking collectives: 29.8 us -> none  [per_device(): total = lax.psum(jnp.sum(floats * floats, axis=1), 'ep')]
    dot_general x17 -> x0, matrix products: 22.2 us -> none  [the longest x4 5.92 us: outgoing(): jnp.dot(picker, projected, preferred_element_type=jnp.float32)]
    all_to_all x5 -> x0, starting transfers between devices: 19.8 us -> none  [the longest x1 5.98 us: per_device(): lax.all_to_all(send_query, 'ep', split_axis=0, concat_axis=0, tiled=True)]
    all_to_all x5 -> x0, waiting for transfers between devices: 17.5 us -> none  [the longest x1 6.42 us: per_device(): lax.all_to_all(expert_rows, 'ep', split_axis=1, concat_axis=0, tiled=True)]
    unnamed x21 -> x6, local copies, waits for them, and re-layouts: 3.27 us -> 12.3 us
    add x1 -> x0, other arithmetic: 2.74 us -> none  [per_device(): head_states * jnp.exp(log_decay)[:, :, None]]
  transfers between devices with their start and end apart: 5 -> 0, of which waited for: 3 -> 0; matrix products, arithmetic and copies ran while one was open for 12% -> 0% of each run, Pallas kernels for 0% -> 0%
where the time goes in v1:
time: 54 us; the launch traced here: 53.6 us
  Pallas kernels  36.8 us (68%)
  local copies, waits for them, and re-layouts  16.2 us (30%)
  between operations  0.64 us (1%)
    pallas_call x1, Pallas kernels, per_device(): pl.pallas_call(functools.partial(kernel_body, n), out_shape=(jax.ShapeDty...  36.8 us
    unnamed x6, local copies, waits for them, and re-layouts  12.3 us
    reshape x3, local copies, waits for them, and re-layouts, per_device(): args[i] = args[i].reshape(1, -1)  3.9 us

profile of v1, /device:TPU:0, one launch (start us, length us, event | category | flops | bytes accessed | tf_op | source)
XLA Modules:
  0.0 53.6 jit_solution(14078408894194021085)
XLA Ops:
  0.6 1.3 %reshape.18.refs_10_ = bf16[1,1024]{1,0:T(2,128)(2,1)} reshape(bf16[1024]{0:T(1024)(128)(2,1)} %param.29) | data formatting | bytes 4096 | tf_op jit(solution)/shard_map/reshape | solution.py:382
  1.9 1.3 %copy.22.refs_13_ = s32[8,2]{1,0:T(8,128)} copy(s32[8,2]{0,1:T(2,128)} %param.32) | data formatting | bytes 128 | tf_op args[13]
  3.3 1.3 %copy.23.refs_14_ = f32[8,4]{1,0:T(8,128)} copy(f32[8,4]{0,1:T(4,128)} %param.33) | data formatting | bytes 256 | tf_op args[14]
  4.6 1.3 %copy.24.refs_15_ = f32[8,2]{1,0:T(8,128)} copy(f32[8,2]{0,1:T(2,128)} %param.34) | data formatting | bytes 128 | tf_op args[15]
  5.9 1.3 %reshape.16.refs_2_ = bf16[1,4096]{1,0:T(2,128)(2,1)} reshape(bf16[4096]{0:T(1024)(128)(2,1)} %param.21) | data formatting | bytes 16384 | tf_op jit(solution)/shard_map/reshape | solution.py:382
  7.2 1.3 %reshape.19.refs_12_ = bf16[1,4096]{1,0:T(2,128)(2,1)} reshape(bf16[4096]{0:T(1024)(128)(2,1)} %param.31) | data formatting | bytes 16384 | tf_op jit(solution)/shard_map/reshape | solution.py:382
  8.6 2.2 %copy.21.refs_7_ = bf16[4096,16]{1,0:T(8,128)(2,1)} copy(bf16[4096,16]{0,1:T(8,128)(2,1)} %param.26) | data formatting | bytes 262144 | tf_op args[7]
  10.8 36.8 %layer.1 = (bf16[8,256]{1,0:T(8,128)(2,1)}, f32[2,512,1024]{2,1,0:T(8,128)}) custom-call(bf16[8,256]{1,0:T(8,128)(2,1)} %refs_0_.1, f32[2,512,1024]{2,1,0:T(8,128)} %refs_1_.1, bf16[1,4096]{1,0:T(2,128)(2,1)} %reshape.16.refs_2_, bf16[4096,128]{1,0:T(8,128)(2,1)} %refs_3_.1, bf16[4096,128]{1,0:T(8,128)(2,1)} %refs_4_.1, bf16[4096,256]{1,0:T(8,128)(2,1)} %refs_5_.1, ...), custom_call_target="tpu_custom_call" | custom-call | tf_op jit(solution)/shard_map/layer/pallas_call | solution.py:393
  47.6 1.3 %copy.27 = bf16[8,256]{1,0:T(8,128)(2,1)} copy(bf16[8,256]{1,0:T(8,128)(2,1)} %get-tuple-element.4) | data formatting | bytes 8192
  48.8 4.8 %copy.28 = f32[2,512,1024]{2,1,0:T(8,128)} copy(f32[2,512,1024]{2,1,0:T(8,128)} %get-tuple-element.5) | data formatting | bytes 8388608

commit v2 on v1

--- a/solution.py
+++ b/solution.py
@@ -43,7 +43,6 @@
         layer_out,
         new_states,
         res_v,
-        states_v,
         gain1_v,
         wq_v,
         wk_v,
@@ -73,9 +72,7 @@
         gath4,
         send5,
         recv5,
-        out_v,
         local_sem,
-        out_sem,
         s1,
         r1,
         s2,
@@ -87,6 +84,7 @@
         s5,
         r5,
     ) = refs
+    states_v = new_states
     me = lax.axis_index("ep")
     seqs, own = residual.shape
     width = own * n
@@ -180,8 +178,12 @@
             x = gath[s].astype(F32)
             total = total + x * x
         scale = lax.rsqrt(jnp.sum(total, axis=1, keepdims=True) / width + NORM_EPS)
+        gains = gain[...].astype(F32)
+        per = own // 128
         for s in range(n):
-            g = gain[:, s * own : (s + 1) * own].astype(F32)
+            g = jnp.concatenate(
+                [gains[s * per + c : s * per + c + 1, :] for c in range(per)], axis=1
+            )
             lhs[:, s * own : (s + 1) * own] = (gath[s].astype(F32) * scale * g).astype(BF16)
 
     normalise(gath1, gain1_v)
@@ -234,7 +236,9 @@
             pltpu.make_async_copy(send2.at[s], recv2.at[my_slot], r2.at[my_slot]).start()
 
     staged(6, 7, 8)
-    (low,) = kdot((wlow_v,), 1024)
+    low = lax.dot_general(
+        lhs[...], wlow_v[...], (((1,), (1,)), ((), ())), preferred_element_type=F32
+    )
     head_at = pl.ds(pl.multiple_of(my_head0 * DK, DK), pairs_dev * DK)
     pre = jnp.dot(
         low,
@@ -265,6 +269,11 @@
         for i in range(dph):
             out.extend(lanes(p * dph + i, start, size))
         return jnp.concatenate(out, axis=1)
+
+    def folded(row):
+        return jnp.concatenate(
+            [row[:, c * 128 : (c + 1) * 128] for c in range(row.shape[1] // 128)], axis=0
+        )
 
     stack = []
     for p in range(pairs_dev):
@@ -288,12 +297,12 @@
             return acc + jnp.sum(weighted.reshape(step_rows // 8, 8, DV), axis=0)
 
         acc = lax.fori_loop(0, DK // step_rows, update, jnp.zeros((8, DV), F32))
-        pltpu.make_async_copy(states_v.at[p], new_states.at[p], out_sem.at[p]).start()
         read = jnp.sum(acc, axis=0, keepdims=True)
-        gate = gathered_row(p, 2 * qw + vw, vw)
         scale = lax.rsqrt(jnp.mean(read * read, axis=1, keepdims=True) + NORM_EPS)
+        read = folded(read)
+        gate = folded(gathered_row(p, 2 * qw + vw, vw))
         mixed = read * scale * hgain_v[...].astype(F32) * (gate / (1.0 + jnp.exp(-gate)))
-        mixed_rows.extend(mixed[:, c * 128 : (c + 1) * 128] for c in range(DV // 128))
+        mixed_rows.append(mixed)
     send3[...] = jnp.concatenate(mixed_rows, axis=0).astype(BF16)
 
     spread(send3, gath3.at[me], s3, r3)
@@ -315,14 +324,18 @@
     gath4[me] = stream
     staged(12, 13, 14, 15)
     group_exp = jnp.exp(glog_v[...])
-    group_prob = group_exp / jnp.sum(group_exp, axis=1, keepdims=True)
+    group_prob = group_exp / jnp.sum(group_exp, axis=0, keepdims=True)
     route = routes_v[...]
-    chosen = route[:, 0:1] // (n // GROUPS)
-    group_is = lax.broadcasted_iota(jnp.int32, group_prob.shape, 1) == chosen
-    picked = jnp.sum(jnp.where(group_is, group_prob, 0.0), axis=1, keepdims=True)
+    chosen = route[0:1, :] // (n // GROUPS)
+    group_is = lax.broadcasted_iota(jnp.int32, group_prob.shape, 0) == chosen
+    picked = jnp.sum(jnp.where(group_is, group_prob, 0.0), axis=0, keepdims=True)
     expert_exp = jnp.exp(elog_v[...])
-    weights = expert_exp / jnp.sum(expert_exp, axis=1, keepdims=True) * picked
-    mine = jnp.sum(jnp.where(route == me, weights, 0.0), axis=1, keepdims=True)
+    weights = expert_exp / jnp.sum(expert_exp, axis=0, keepdims=True) * picked
+    mine = jnp.sum(jnp.where(route == me, weights, 0.0), axis=0, keepdims=True)
+    diagonal = lax.broadcasted_iota(jnp.int32, (seqs, seqs), 0) == lax.broadcasted_iota(
+        jnp.int32, (seqs, seqs), 1
+    )
+    mine = jnp.sum(jnp.where(diagonal, mine, 0.0), axis=1, keepdims=True)
     drain(stream_v, gath4, s4, r4)
     normalise(gath4, gain2_v)
     staged(16, 17)
@@ -355,9 +368,7 @@
     total = jnp.zeros((seqs, own), F32)
     for s in range(n):
         total = total + recv5[s].astype(F32)
-    out_v[...] = (stream.astype(F32) + total).astype(BF16)
-    out_copy = pltpu.make_async_copy(out_v, layer_out, out_sem.at[pairs_dev])
-    out_copy.start()
+    layer_out[...] = (stream.astype(F32) + total).astype(BF16)
 
     drain_sends(res_v, gath1, s1)
     drain_sends(send3, gath3, s3)
@@ -370,16 +381,16 @@
         def _():
             copy2(s).wait_send()
 
-    for p in range(pairs_dev):
-        pltpu.make_async_copy(states_v.at[p], new_states.at[p], out_sem.at[p]).wait()
-    out_copy.wait()
-
 
 def per_device(*args):
     n = lax.axis_size("ep")
     args = list(args)
-    for i in (2, 9, 10, 12):
-        args[i] = args[i].reshape(1, -1)
+    for i in (2, 10, 12):
+        args[i] = args[i].reshape(-1, 128)
+    args[9] = args[9].reshape(1, -1)
+    for i in (7, 13, 14, 15):
+        args[i] = args[i].T
+    args = [pltpu.with_memory_space_constraint(a, pltpu.HBM) for a in args]
     residual, head_states = args[0], args[1]
     seqs, own = residual.shape
     pairs_dev = head_states.shape[0]
@@ -389,15 +400,15 @@
     tiles2 = (2 * qw + 2 * vw) // 128
     rows3 = pairs_dev * DV // 128
     dma = pltpu.SemaphoreType.DMA
-    stage = [pltpu.VMEM(a.shape, a.dtype) for a in args]
+    stage = [pltpu.VMEM(a.shape, a.dtype) for i, a in enumerate(args) if i != 1]
     return pl.pallas_call(
         functools.partial(kernel_body, n),
         out_shape=(
-            jax.ShapeDtypeStruct(residual.shape, BF16),
-            jax.ShapeDtypeStruct(head_states.shape, F32),
+            pltpu.VMEM(residual.shape, BF16),
+            pltpu.VMEM(head_states.shape, F32),
         ),
-        in_specs=[pl.BlockSpec(memory_space=pl.ANY)] * len(args),
-        out_specs=(pl.BlockSpec(memory_space=pl.ANY),) * 2,
+        in_specs=[pl.BlockSpec(memory_space=pltpu.HBM)] * len(args),
+        out_specs=(pl.BlockSpec(memory_space=pltpu.VMEM),) * 2,
         scratch_shapes=stage
         + [
             pltpu.VMEM((n, seqs, own), BF16),
@@ -412,9 +423,7 @@
             pltpu.VMEM((n, seqs, own), BF16),
             pltpu.VMEM((n, seqs, own), BF16),
             pltpu.VMEM((n, seqs, own), BF16),
-            pltpu.VMEM((seqs, own), BF16),
             dma((len(args),)),
-            dma((pairs_dev + 1,)),
             dma((n,)),
             dma((n,)),
             dma((seqs,)),
@@ -427,7 +436,7 @@
             dma((n,)),
         ],
         compiler_params=pltpu.CompilerParams(
-            collective_id=0, has_side_effects=True, vmem_limit_bytes=56 * 1024 * 1024
+            collective_id=0, has_side_effects=True, vmem_limit_bytes=48 * 1024 * 1024
         ),
         name="layer",
     )(*args)

time: 54 us -> 40.1 us (0.74)
  local copies, waits for them, and re-layouts: 16.2 us -> 2.61 us
    unnamed x6 -> x2, local copies, waits for them, and re-layouts: 12.3 us -> 2.61 us
    reshape x3 -> x0, local copies, waits for them, and re-layouts: 3.9 us -> none  [per_device(): args[i] = args[i].reshape(1, -1)]
where the time goes in v2:
time: 40.1 us; the launch traced here: 40 us
  Pallas kernels  36.7 us (92%)
  local copies, waits for them, and re-layouts  2.61 us (7%)
  between operations  0.65 us (2%)
    pallas_call x1, Pallas kernels, per_device(): pl.pallas_call(functools.partial(kernel_body, n), out_shape=(pltpu.VMEM(r...  36.7 us
    unnamed x2, local copies, waits for them, and re-layouts  2.61 us

profile of v2, /device:TPU:0, one launch (start us, length us, event | category | flops | bytes accessed | tf_op | source)
XLA Modules:
  0.0 40.0 jit_solution(12739756660998352275)
XLA Ops:
  0.6 36.7 %layer.1 = (bf16[8,256]{1,0:T(8,128)(2,1)S(1)}, f32[2,512,1024]{2,1,0:T(8,128)S(1)}) custom-call(bf16[8,256]{1,0:T(8,128)(2,1)} %refs_0_.1, f32[2,512,1024]{2,1,0:T(8,128)} %refs_1_.1, bf16[32,128]{1,0:T(8,128)(2,1)} %bitcast.9, bf16[4096,128]{1,0:T(8,128)(2,1)} %refs_3_.1, bf16[4096,128]{1,0:T(8,128)(2,1)} %refs_4_.1, bf16[4096,256]{1,0:T(8,128)(2,1)} %refs_5_.1, ...), custom_call_target="tpu_custom_call" | custom-call | tf_op jit(solution)/shard_map/layer/pallas_call | solution.py:404
  37.3 0.6 %copy.23 = bf16[8,256]{1,0:T(8,128)(2,1)} copy(bf16[8,256]{1,0:T(8,128)(2,1)S(1)} %get-tuple-element.2) | data formatting | bytes 8192
  37.9 2.0 %copy.24 = f32[2,512,1024]{2,1,0:T(8,128)} copy(f32[2,512,1024]{2,1,0:T(8,128)S(1)} %get-tuple-element.3) | data formatting | bytes 8388608

commit v3 on v2

--- a/solution.py
+++ b/solution.py
@@ -68,6 +68,8 @@
         send3,
         gath3,
         stage3,
+        gain1_f,
+        gain2_f,
         stream_v,
         gath4,
         send5,
@@ -140,70 +142,62 @@
     staged(0)
     pl.semaphore_wait(barrier, n - 1)
 
-    def spread(src, dst_of_me, send_sem, recv_sem):
-        def one(o):
-            t = lax.rem(me + o, n)
-            return pltpu.make_async_remote_copy(
-                src_ref=src,
-                dst_ref=dst_of_me,
-                send_sem=send_sem.at[o],
-                recv_sem=recv_sem.at[me],
-                device_id={"ep": t},
-                device_id_type=MESH,
-            )
-
-        @pl.loop(1, n)
-        def _(o):
-            one(o).start()
-
-    def drain(src, buffer, send_sem, recv_sem):
-        @pl.loop(1, n)
-        def _(o):
-            s = lax.rem(me + o, n)
-            pltpu.make_async_copy(src, buffer.at[s], recv_sem.at[s]).wait()
-
-    def drain_sends(src, buffer, send_sem):
-        @pl.loop(1, n)
-        def _(o):
-            pltpu.make_async_copy(src, buffer.at[0], send_sem.at[o]).wait()
-
-    spread(res_v, gath1.at[me], s1, r1)
+    bit_count = n.bit_length() - 1
+    signs = [1 - 2 * lax.rem(me // 2**b, 2) for b in range(bit_count)]
+
+    def partner_of(o):
+        if 2**bit_count != n:
+            return lax.rem(me + o, n)
+        return me + sum(signs[b] * 2**b for b in range(bit_count) if o >> b & 1)
+
+    partner = [partner_of(o) for o in range(n)]
+    far_first = range(n - 1, 0, -1)
+
+    def send(src, dst, send_sem, recv_sem, target):
+        pltpu.make_async_remote_copy(
+            src_ref=src,
+            dst_ref=dst,
+            send_sem=send_sem,
+            recv_sem=recv_sem,
+            device_id={"ep": target},
+            device_id_type=MESH,
+        ).start()
+
+    def wait_blocks(buffer, sem):
+        part = buffer.at[pl.ds(0, n - 1)]
+        pltpu.make_async_copy(part, part, sem).wait()
+
+    per = own // 128
+    own_at = [pl.ds(pl.multiple_of(t * own, own), own) for t in partner]
+
+    def absorb(gath, recv_sem, gains, weights, keep):
+        accs = [jnp.zeros((seqs, w.shape[-1]), F32) for w in weights]
+        total = jnp.zeros((seqs, own), F32)
+        for o in range(n):
+            t = partner[o]
+            if o:
+                block = gath.at[t]
+                pltpu.make_async_copy(block, block, recv_sem.at[t]).wait()
+            x = gath[t].astype(F32)
+            total = total + x * x
+            gain = jnp.concatenate([gains[pl.ds(t * per + c, 1), :] for c in range(per)], axis=1)
+            x = (x * gain).astype(BF16)
+            if keep:
+                lhs[:, own_at[o]] = x
+            accs = [
+                acc + jnp.dot(x, w[own_at[o], :], preferred_element_type=F32)
+                for acc, w in zip(accs, weights)
+            ]
+        scale = lax.rsqrt(jnp.sum(total, axis=1, keepdims=True) / width + NORM_EPS)
+        return scale, [acc * scale for acc in accs]
+
+    for o in far_first:
+        send(res_v, gath1.at[me], s1.at[0], r1.at[me], partner[o])
     gath1[me] = res_v[...]
-    drain(res_v, gath1, s1, r1)
     staged(1)
-
-    def normalise(gath, gain):
-        total = jnp.zeros((seqs, own), F32)
-        for s in range(n):
-            x = gath[s].astype(F32)
-            total = total + x * x
-        scale = lax.rsqrt(jnp.sum(total, axis=1, keepdims=True) / width + NORM_EPS)
-        gains = gain[...].astype(F32)
-        per = own // 128
-        for s in range(n):
-            g = jnp.concatenate(
-                [gains[s * per + c : s * per + c + 1, :] for c in range(per)], axis=1
-            )
-            lhs[:, s * own : (s + 1) * own] = (gath[s].astype(F32) * scale * g).astype(BF16)
-
-    normalise(gath1, gain1_v)
-
-    def kdot(weights, chunk):
-        depth = lhs.shape[1]
-        outs = tuple(jnp.zeros((seqs, w.shape[1]), F32) for w in weights)
-
-        def step(i, accs):
-            at = pl.ds(pl.multiple_of(i * chunk, chunk), chunk)
-            x = lhs[:, at]
-            return tuple(
-                acc + jnp.dot(x, w[at, :], preferred_element_type=F32)
-                for acc, w in zip(accs, weights)
-            )
-
-        return lax.fori_loop(0, depth // chunk, step, outs)
-
+    gain1_f[...] = gain1_v[...].astype(F32)
     staged(2, 3, 4, 5)
-    q, k, v, g = kdot((wq_v, wk_v, wv_v, wg_v), 512)
+    scale1, (q, k, v, g) = absorb(gath1, r1, gain1_f, (wq_v, wk_v, wv_v, wg_v), True)
     row = jnp.concatenate([q, k, v, g], axis=1).astype(BF16).astype(F32)
     for c in range(tiles2):
         part = row[:, c * 128 : (c + 1) * 128]
@@ -236,7 +230,7 @@
             pltpu.make_async_copy(send2.at[s], recv2.at[my_slot], r2.at[my_slot]).start()
 
     staged(6, 7, 8)
-    low = lax.dot_general(
+    low = scale1 * lax.dot_general(
         lhs[...], wlow_v[...], (((1,), (1,)), ((), ())), preferred_element_type=F32
     )
     head_at = pl.ds(pl.multiple_of(my_head0 * DK, DK), pairs_dev * DK)
@@ -275,29 +269,34 @@
             [row[:, c * 128 : (c + 1) * 128] for c in range(row.shape[1] // 128)], axis=0
         )
 
-    stack = []
+    stack, overlap = [], []
     for p in range(pairs_dev):
-        stack.append(gathered_row(p, 0, qw) * DK ** (-0.5))
-        stack.append(gathered_row(p, qw, qw))
-        stack.append(decay[:, p * DK : (p + 1) * DK])
+        query = gathered_row(p, 0, qw) * DK ** (-0.5)
+        key = gathered_row(p, qw, qw)
+        fade = decay[:, p * DK : (p + 1) * DK]
+        stack.extend([query * fade, key, fade])
+        overlap.append(jnp.sum(query * key, axis=1, keepdims=True))
     stack.append(jnp.zeros((8 - len(stack), DK), F32))
     cols[...] = jnp.transpose(jnp.concatenate(stack, axis=0))
+    values = [gathered_row(p, 2 * qw, vw) for p in range(pairs_dev)]
     staged(9, 10)
-    step_rows = 32
+    step_rows = 128
+
+    def read_step(i, accs):
+        base = pl.multiple_of(i * step_rows, step_rows)
+        out = []
+        for p, acc in enumerate(accs):
+            fading = cols[pl.ds(base, step_rows), 3 * p : 3 * p + 1]
+            for r in range(0, step_rows, 8):
+                acc = acc + states_v[p, pl.ds(base + r, 8), :] * fading[r : r + 8]
+            out.append(acc)
+        return tuple(out)
+
+    zero = jnp.zeros((8, DV), F32)
+    accs = lax.fori_loop(0, DK // step_rows, read_step, (zero,) * pairs_dev)
     mixed_rows = []
     for p in range(pairs_dev):
-        value = gathered_row(p, 2 * qw, vw)
-
-        def update(i, acc):
-            at = pl.ds(pl.multiple_of(i * step_rows, step_rows), step_rows)
-            three = cols[at, 3 * p : 3 * p + 3]
-            fresh = states_v[p, at, :] * three[:, 2:3] + three[:, 1:2] * value
-            states_v[p, at, :] = fresh
-            weighted = fresh * three[:, 0:1]
-            return acc + jnp.sum(weighted.reshape(step_rows // 8, 8, DV), axis=0)
-
-        acc = lax.fori_loop(0, DK // step_rows, update, jnp.zeros((8, DV), F32))
-        read = jnp.sum(acc, axis=0, keepdims=True)
+        read = jnp.sum(accs[p], axis=0, keepdims=True) + overlap[p] * values[p]
         scale = lax.rsqrt(jnp.mean(read * read, axis=1, keepdims=True) + NORM_EPS)
         read = folded(read)
         gate = folded(gathered_row(p, 2 * qw + vw, vw))
@@ -305,24 +304,24 @@
         mixed_rows.append(mixed)
     send3[...] = jnp.concatenate(mixed_rows, axis=0).astype(BF16)
 
-    spread(send3, gath3.at[me], s3, r3)
+    for o in far_first:
+        send(send3, gath3.at[me], s3.at[0], r3.at[0], partner[o])
     gath3[me] = send3[...]
-    drain(send3, gath3, s3, r3)
-    per_seq = HEADS // pairs_dev
-    for d in range(n):
-        stage3[d // per_seq, (d % per_seq) * rows3 : (d % per_seq + 1) * rows3, :] = gath3[
-            d
-        ].astype(F32)
-    for c in range(HEADS * DV // 128):
-        lhs[:, c * 128 : (c + 1) * 128] = stage3[:, c, :].astype(BF16)
-    staged(11)
-    (branch,) = kdot((wout_v,), 1024)
-    stream = (res_v[...].astype(F32) + branch.astype(BF16).astype(F32)).astype(BF16)
-    stream_v[...] = stream
-
-    spread(stream_v, gath4.at[me], s4, r4)
-    gath4[me] = stream
+
+    @pl.loop(0, DK // step_rows)
+    def _(i):
+        base = pl.multiple_of(i * step_rows, step_rows)
+        for p in range(pairs_dev):
+            keys = cols[pl.ds(base, step_rows), 3 * p + 1 : 3 * p + 2]
+            fades = cols[pl.ds(base, step_rows), 3 * p + 2 : 3 * p + 3]
+            for r in range(0, step_rows, 8):
+                at = pl.ds(base + r, 8)
+                states_v[p, at, :] = (
+                    states_v[p, at, :] * fades[r : r + 8] + keys[r : r + 8] * values[p]
+                )
+
     staged(12, 13, 14, 15)
+    gain2_f[...] = gain2_v[...].astype(F32)
     group_exp = jnp.exp(glog_v[...])
     group_prob = group_exp / jnp.sum(group_exp, axis=0, keepdims=True)
     route = routes_v[...]
@@ -336,50 +335,74 @@
         jnp.int32, (seqs, seqs), 1
     )
     mine = jnp.sum(jnp.where(diagonal, mine, 0.0), axis=1, keepdims=True)
-    drain(stream_v, gath4, s4, r4)
-    normalise(gath4, gain2_v)
-    staged(16, 17)
-    gate_part, up_part = kdot((eg_v.at[0], eu_v.at[0]), 512)
+    others3 = gath3.at[pl.ds(0, n - 1)]
+    pltpu.make_async_copy(others3, others3, r3.at[0]).wait()
+    per_seq = HEADS // pairs_dev
+    for d in range(n):
+        stage3[d // per_seq, (d % per_seq) * rows3 : (d % per_seq + 1) * rows3, :] = gath3[
+            d
+        ].astype(F32)
+    for c in range(HEADS * DV // 128):
+        lhs[:, c * 128 : (c + 1) * 128] = stage3[:, c, :].astype(BF16)
+    staged(11)
+    branch = jnp.dot(lhs[...], wout_v[...], preferred_element_type=F32)
+    stream = (res_v[...].astype(F32) + branch.astype(BF16).astype(F32)).astype(BF16)
+    stream_v[...] = stream
+
+    for o in far_first:
+        send(stream_v, gath4.at[me], s4.at[0], r4.at[me], partner[o])
+    gath4[me] = stream
+    staged(16, 17, 18)
+    _, (gate_part, up_part) = absorb(gath4, r4, gain2_f, (eg_v.at[0], eu_v.at[0]), False)
     active = (gate_part / (1.0 + jnp.exp(-gate_part)) * up_part * mine).astype(BF16)
-    staged(18)
-
-    def copy5(o):
-        t = lax.rem(me + o, n)
-        return pltpu.make_async_remote_copy(
-            src_ref=send5.at[o],
-            dst_ref=recv5.at[me],
-            send_sem=s5.at[o],
-            recv_sem=r5.at[me],
-            device_id={"ep": t},
-            device_id_type=MESH,
-        )
-
-    def contribution(t):
-        at = pl.ds(pl.multiple_of(t * own, own), own)
-        return jnp.dot(active, ed_v[0, :, at], preferred_element_type=F32).astype(BF16)
-
-    @pl.loop(1, n)
-    def _(o):
-        send5[o] = contribution(lax.rem(me + o, n))
-        copy5(o).start()
-
-    recv5[me] = contribution(me)
-    drain(stream_v, recv5, s5, r5)
+
+    def contribution(o):
+        return jnp.dot(active, ed_v[0, :, own_at[o]], preferred_element_type=F32).astype(BF16)
+
+    group = 4
+    for first in range(n - 1, 0, -group):
+        some = range(first, max(first - group, 0), -1)
+        for o in some:
+            send5[o] = contribution(o)
+        for o in some:
+            send(send5.at[o], recv5.at[me], s5.at[0], r5.at[0], partner[o])
+    recv5[me] = contribution(0)
+    wait_blocks(recv5, r5.at[0])
     total = jnp.zeros((seqs, own), F32)
     for s in range(n):
         total = total + recv5[s].astype(F32)
     layer_out[...] = (stream.astype(F32) + total).astype(BF16)
 
-    drain_sends(res_v, gath1, s1)
-    drain_sends(send3, gath3, s3)
-    drain_sends(stream_v, gath4, s4)
-    drain_sends(stream_v, recv5, s5)
+    wait_blocks(gath1, s1.at[0])
+    wait_blocks(gath3, s3.at[0])
+    wait_blocks(gath4, s4.at[0])
+    wait_blocks(recv5, s5.at[0])
 
     @pl.loop(0, seqs)
     def _(s):
         @pl.when(target2(s) != me)
         def _():
             copy2(s).wait_send()
+
+
+PUTS = 4
+
+
+def put_body(layer_out, new_states, layer_hbm, states_hbm, sem):
+    copies = [pltpu.make_async_copy(layer_out, layer_hbm, sem.at[0])]
+    rows = DK // PUTS
+    for p in range(new_states.shape[0]):
+        for i in range(PUTS):
+            at = pl.ds(i * rows, rows)
+            copies.append(
+                pltpu.make_async_copy(
+                    new_states.at[p, at], states_hbm.at[p, at], sem.at[len(copies)]
+                )
+            )
+    for copy in copies:
+        copy.start()
+    for copy in copies:
+        copy.wait()
 
 
 def per_device(*args):
@@ -401,7 +424,7 @@
     rows3 = pairs_dev * DV // 128
     dma = pltpu.SemaphoreType.DMA
     stage = [pltpu.VMEM(a.shape, a.dtype) for i, a in enumerate(args) if i != 1]
-    return pl.pallas_call(
+    results = pl.pallas_call(
         functools.partial(kernel_body, n),
         out_shape=(
             pltpu.VMEM(residual.shape, BF16),
@@ -419,27 +442,38 @@
             pltpu.VMEM((rows3, 128), BF16),
             pltpu.VMEM((n, rows3, 128), BF16),
             pltpu.VMEM((seqs, HEADS * DV // 128, 128), F32),
+            pltpu.VMEM((width // 128, 128), F32),
+            pltpu.VMEM((width // 128, 128), F32),
             pltpu.VMEM((seqs, own), BF16),
             pltpu.VMEM((n, seqs, own), BF16),
             pltpu.VMEM((n, seqs, own), BF16),
             pltpu.VMEM((n, seqs, own), BF16),
             dma((len(args),)),
-            dma((n,)),
+            dma((1,)),
             dma((n,)),
             dma((seqs,)),
             dma((group_src,)),
+            dma((1,)),
+            dma((1,)),
+            dma((1,)),
             dma((n,)),
-            dma((n,)),
-            dma((n,)),
-            dma((n,)),
-            dma((n,)),
-            dma((n,)),
+            dma((1,)),
+            dma((1,)),
         ],
         compiler_params=pltpu.CompilerParams(
             collective_id=0, has_side_effects=True, vmem_limit_bytes=48 * 1024 * 1024
         ),
         name="layer",
     )(*args)
+    return pl.pallas_call(
+        put_body,
+        out_shape=tuple(jax.ShapeDtypeStruct(a.shape, a.dtype) for a in (residual, head_states)),
+        in_specs=[pl.BlockSpec(memory_space=pltpu.VMEM)] * 2,
+        out_specs=(pl.BlockSpec(memory_space=pltpu.HBM),) * 2,
+        scratch_shapes=[dma((1 + pairs_dev * PUTS,))],
+        compiler_params=pltpu.CompilerParams(vmem_limit_bytes=1024 * 1024),
+        name="put",
+    )(*results)
 
 
 def solution(mesh):

time: 40.1 us -> 33.4 us (0.83)
  Pallas kernels: 36.7 us -> 32.6 us
  local copies, waits for them, and re-layouts: 2.61 us -> 0 us
    pallas_call x1, Pallas kernels: 36.7 us -> 30.5 us  [per_device(): pl.pallas_call(functools.partial(kernel_body, n), out_shape=(pltpu.VMEM(r...]
    unnamed x2 -> x0, local copies, waits for them, and re-layouts: 2.61 us -> none
    pallas_call x0 -> x1, Pallas kernels: none -> 2.08 us  [per_device(): pl.pallas_call(put_body, out_shape=tuple((jax.ShapeDtypeStruct(a.shape, a...]
where the time goes in v3:
time: 33.4 us; the launch traced here: 33.2 us
  Pallas kernels  32.6 us (98%)
  between operations  0.65 us (2%)
    pallas_call x1, Pallas kernels, per_device(): pl.pallas_call(functools.partial(kernel_body, n), out_shape=(pltpu.VMEM(r...  30.5 us
    pallas_call x1, Pallas kernels, per_device(): pl.pallas_call(put_body, out_shape=tuple((jax.ShapeDtypeStruct(a.shape, a...  2.08 us

profile of v3, /device:TPU:0, one launch (start us, length us, event | category | flops | bytes accessed | tf_op | source)
XLA Modules:
  0.0 33.2 jit_solution(16269538393166376427)
XLA Ops:
  0.6 30.5 %layer.1 = (bf16[8,256]{1,0:T(8,128)(2,1)S(1)}, f32[2,512,1024]{2,1,0:T(8,128)S(1)}) custom-call(bf16[8,256]{1,0:T(8,128)(2,1)} %refs_0_.1, f32[2,512,1024]{2,1,0:T(8,128)} %refs_1_.1, bf16[32,128]{1,0:T(8,128)(2,1)} %bitcast.9, bf16[4096,128]{1,0:T(8,128)(2,1)} %refs_3_.1, bf16[4096,128]{1,0:T(8,128)(2,1)} %refs_4_.1, bf16[4096,256]{1,0:T(8,128)(2,1)} %refs_5_.1, ...), custom_call_target="tpu_custom_call" | custom-call | tf_op jit(solution)/shard_map/layer/pallas_call | solution.py:427
  31.1 2.1 %put.1 = (bf16[8,256]{1,0:T(8,128)(2,1)}, f32[2,512,1024]{2,1,0:T(8,128)}) custom-call(bf16[8,256]{1,0:T(8,128)(2,1)S(1)} %get-tuple-element.4.layer_out, f32[2,512,1024]{2,1,0:T(8,128)S(1)} %get-tuple-element.5.new_states), custom_call_target="tpu_custom_call" | custom-call | tf_op jit(solution)/shard_map/put/pallas_call | solution.py:468

commit v4 on v3

--- a/solution.py
+++ b/solution.py
@@ -100,6 +100,23 @@
     tiles2 = send2.shape[1]
     rows3 = send3.shape[0]
 
+    bit_count = n.bit_length() - 1
+    signs = [1 - 2 * lax.rem(me // 2**b, 2) for b in range(bit_count)]
+
+    def partner_of(o):
+        if 2**bit_count != n:
+            return lax.rem(me + o, n)
+        return me + sum(signs[b] * 2**b for b in range(bit_count) if o >> b & 1)
+
+    partner = [partner_of(o) for o in range(n)]
+    far_first = range(n - 1, 0, -1)
+
+    barrier = pltpu.get_barrier_semaphore()
+    for o in far_first:
+        pl.semaphore_signal(
+            barrier, inc=1, device_id={"ep": partner[o]}, device_id_type=MESH
+        )
+
     pieces = [
         (residual, res_v),
         (first_gain, gain1_v),
@@ -124,34 +141,15 @@
     copies = [
         pltpu.make_async_copy(src, dst, local_sem.at[i]) for i, (src, dst) in enumerate(pieces)
     ]
-    for copy in copies:
+    for copy in copies[:9]:
         copy.start()
 
     def staged(*indices):
         for i in indices:
             copies[i].wait()
 
-    barrier = pltpu.get_barrier_semaphore()
-
-    @pl.loop(1, n)
-    def _(o):
-        pl.semaphore_signal(
-            barrier, inc=1, device_id={"ep": lax.rem(me + o, n)}, device_id_type=MESH
-        )
-
     staged(0)
     pl.semaphore_wait(barrier, n - 1)
-
-    bit_count = n.bit_length() - 1
-    signs = [1 - 2 * lax.rem(me // 2**b, 2) for b in range(bit_count)]
-
-    def partner_of(o):
-        if 2**bit_count != n:
-            return lax.rem(me + o, n)
-        return me + sum(signs[b] * 2**b for b in range(bit_count) if o >> b & 1)
-
-    partner = [partner_of(o) for o in range(n)]
-    far_first = range(n - 1, 0, -1)
 
     def send(src, dst, send_sem, recv_sem, target):
         pltpu.make_async_remote_copy(
@@ -168,26 +166,34 @@
         pltpu.make_async_copy(part, part, sem).wait()
 
     per = own // 128
+    group_sizes = [4] * (n // 4 - 1) + [n % 4 + 2, 2]
     own_at = [pl.ds(pl.multiple_of(t * own, own), own) for t in partner]
 
     def absorb(gath, recv_sem, gains, weights, keep):
         accs = [jnp.zeros((seqs, w.shape[-1]), F32) for w in weights]
         total = jnp.zeros((seqs, own), F32)
-        for o in range(n):
-            t = partner[o]
-            if o:
-                block = gath.at[t]
-                pltpu.make_async_copy(block, block, recv_sem.at[t]).wait()
-            x = gath[t].astype(F32)
-            total = total + x * x
-            gain = jnp.concatenate([gains[pl.ds(t * per + c, 1), :] for c in range(per)], axis=1)
-            x = (x * gain).astype(BF16)
-            if keep:
-                lhs[:, own_at[o]] = x
-            accs = [
-                acc + jnp.dot(x, w[own_at[o], :], preferred_element_type=F32)
-                for acc, w in zip(accs, weights)
-            ]
+        start = 0
+        for size in group_sizes:
+            some = range(start, start + size)
+            start += size
+            for o in some:
+                if o:
+                    block = gath.at[partner[o]]
+                    pltpu.make_async_copy(block, block, recv_sem.at[partner[o]]).wait()
+            for o in some:
+                t = partner[o]
+                x = gath[t].astype(F32)
+                total = total + x * x
+                gain = jnp.concatenate(
+                    [gains[pl.ds(t * per + c, 1), :] for c in range(per)], axis=1
+                )
+                x = (x * gain).astype(BF16)
+                if keep:
+                    lhs[:, own_at[o]] = x
+                accs = [
+                    acc + jnp.dot(x, w[own_at[o], :], preferred_element_type=F32)
+                    for acc, w in zip(accs, weights)
+                ]
         scale = lax.rsqrt(jnp.sum(total, axis=1, keepdims=True) / width + NORM_EPS)
         return scale, [acc * scale for acc in accs]
 
@@ -197,6 +203,8 @@
     staged(1)
     gain1_f[...] = gain1_v[...].astype(F32)
     staged(2, 3, 4, 5)
+    for copy in copies[9:]:
+        copy.start()
     scale1, (q, k, v, g) = absorb(gath1, r1, gain1_f, (wq_v, wk_v, wv_v, wg_v), True)
     row = jnp.concatenate([q, k, v, g], axis=1).astype(BF16).astype(F32)
     for c in range(tiles2):
@@ -359,7 +367,7 @@
     def contribution(o):
         return jnp.dot(active, ed_v[0, :, own_at[o]], preferred_element_type=F32).astype(BF16)
 
-    group = 4
+    group = 8
     for first in range(n - 1, 0, -group):
         some = range(first, max(first - group, 0), -1)
         for o in some:

time: 33.4 us -> 33.4 us (level)
  no operation moved by 1% of the time
where the time goes in v4:
time: 33.4 us; the launch traced here: 33.2 us
  Pallas kernels  32.6 us (98%)
  between operations  0.65 us (2%)
    pallas_call x1, Pallas kernels, per_device(): pl.pallas_call(functools.partial(kernel_body, n), out_shape=(pltpu.VMEM(r...  30.5 us
    pallas_call x1, Pallas kernels, per_device(): pl.pallas_call(put_body, out_shape=tuple((jax.ShapeDtypeStruct(a.shape, a...  2.08 us

profile of v4, /device:TPU:0, one launch (start us, length us, event | category | flops | bytes accessed | tf_op | source)
XLA Modules:
  0.0 33.2 jit_solution(289469565659081662)
XLA Ops:
  0.6 30.5 %layer.1 = (bf16[8,256]{1,0:T(8,128)(2,1)S(1)}, f32[2,512,1024]{2,1,0:T(8,128)S(1)}) custom-call(bf16[8,256]{1,0:T(8,128)(2,1)} %refs_0_.1, f32[2,512,1024]{2,1,0:T(8,128)} %refs_1_.1, bf16[32,128]{1,0:T(8,128)(2,1)} %bitcast.9, bf16[4096,128]{1,0:T(8,128)(2,1)} %refs_3_.1, bf16[4096,128]{1,0:T(8,128)(2,1)} %refs_4_.1, bf16[4096,256]{1,0:T(8,128)(2,1)} %refs_5_.1, ...), custom_call_target="tpu_custom_call" | custom-call | tf_op jit(solution)/shard_map/layer/pallas_call | solution.py:435
  31.1 2.1 %put.1 = (bf16[8,256]{1,0:T(8,128)(2,1)}, f32[2,512,1024]{2,1,0:T(8,128)}) custom-call(bf16[8,256]{1,0:T(8,128)(2,1)S(1)} %get-tuple-element.4.layer_out, f32[2,512,1024]{2,1,0:T(8,128)S(1)} %get-tuple-element.5.new_states), custom_call_target="tpu_custom_call" | custom-call | tf_op jit(solution)/shard_map/put/pallas_call | solution.py:476
